TPU v7x, 32 devices: a whole 2x2x4 slice. The times are simulated.
32 devices in a mesh: gr: 2 (over x), fs: 8 (over z, y), tp: 2 (over core).
Axes of the slice: x: 2, y: 2, z: 4, core: 2. Of those that a mesh axis runs over, the one named last changes fastest.
Arguments:
- tokens: bfloat16 [2816, 2048], P(('gr', 'fs')), may hold values from -6 to 6
- expert_ids: int32 [2816, 8], P(('gr', 'fs')), may hold values from 0 to 15, all different within a row; in each aligned block of 176 rows (0 to 175, 176 to 351, ...) at most 110 rows name the same one
- route_weight: float32 [2816, 8], P(('gr', 'fs')), may hold values from 0.05 to 1
- norm_gain: float32 [2048], P('tp'), may hold values from 0.1 to 1.9
- expert_gate: float32 [16, 512, 2048], P('gr', 'fs', 'tp'), may hold values from -0.125 to 0.125
- expert_up: float32 [16, 512, 2048], P('gr', 'fs', 'tp'), may hold values from -0.125 to 0.125
- expert_down: float32 [16, 512, 2048], P('gr', 'fs', 'tp'), may hold values from -0.25 to 0.25
- shared_gate: float32 [512, 2048], P('fs', 'tp'), may hold values from -0.125 to 0.125
- shared_up: float32 [512, 2048], P('fs', 'tp'), may hold values from -0.125 to 0.125
- shared_down: float32 [512, 2048], P('fs', 'tp'), may hold values from -0.25 to 0.25
Outputs:
- mixed: bfloat16 [2816, 2048], P(('gr', 'fs'), 'tp')
- new_gate: bfloat16 [2, 8, 512, 2048], P(None, 'fs', None, 'tp')
- new_up: bfloat16 [2, 8, 512, 2048], P(None, 'fs', None, 'tp')
- new_down: bfloat16 [2, 8, 512, 2048], P(None, 'fs', None, 'tp')
- new_shared_gate: bfloat16 [512, 2048], P(None, 'tp')
- new_shared_up: bfloat16 [512, 2048], P(None, 'tp')
- new_shared_down: bfloat16 [512, 2048], P(None, 'tp')
Inputs may be any that keep to these rules, and one draw needn't show every extreme that they name: `expert_ids`: each row names 8 different experts; within each aligned block of 176 rows no expert is named by more than 110 rows, a bound that some block reaches.
All inputs are finite; a program needn't handle non-finite values.
Results may differ from a plain program's by a relative error of at most 0.022.
Values may be sent and summed in bfloat16 or wider, within the bound.
A program may use at most 128 MiB of HBM per device.

v0:
```python
import jax
import jax.numpy as jnp
from jax import lax
from jax.sharding import PartitionSpec as P

route_scale = 2.5
norm_eps = 1e-06


def fold_gain(weight, gain):
    return (weight * gain).astype(jnp.bfloat16)


def body(
    tokens,
    expert_ids,
    route_weight,
    norm_gain,
    expert_gate,
    expert_up,
    expert_down,
    shared_gate,
    shared_up,
    shared_down,
):
    group_count = lax.axis_size("gr")
    shard_count = lax.axis_size("fs")
    column_count = lax.axis_size("tp")
    tok_rows = tokens.shape[0]
    col_width = expert_gate.shape[2]
    top_count = expert_ids.shape[1]
    hidden = expert_gate.shape[1] * shard_count
    shared_hidden = shared_gate.shape[0] * shard_count
    experts = group_count * shard_count
    capacity = tok_rows * top_count * 5 // (4 * experts)
    gate_round = fold_gain(expert_gate, norm_gain)
    up_round = fold_gain(expert_up, norm_gain)
    down_round = expert_down.astype(jnp.bfloat16)
    moved = (
        lax.all_to_all(gate_round, "fs", split_axis=0, concat_axis=1, tiled=True),
        lax.all_to_all(up_round, "fs", split_axis=0, concat_axis=1, tiled=True),
        lax.all_to_all(down_round, "fs", split_axis=0, concat_axis=1, tiled=True),
    )
    whole = (
        lax.all_gather(moved[0], "gr", axis=0, tiled=True),
        lax.all_gather(moved[1], "gr", axis=0, tiled=True),
        lax.all_gather(moved[2], "gr", axis=0, tiled=True),
    )
    new_gate, new_up, new_down = tuple(
        (matrix.reshape(group_count, 1, hidden, col_width) for matrix in whole)
    )
    new_shared_gate, new_shared_up, new_shared_down = (
        lax.all_gather(fold_gain(shared_gate, norm_gain), "fs", axis=0, tiled=True),
        lax.all_gather(fold_gain(shared_up, norm_gain), "fs", axis=0, tiled=True),
        lax.all_gather(shared_down.astype(jnp.bfloat16), "fs", axis=0, tiled=True),
    )
    tok_float = tokens.astype(jnp.float32)
    normed = (
        tok_float * lax.rsqrt(jnp.mean(tok_float * tok_float, axis=1, keepdims=True) + norm_eps)
    ).astype(jnp.bfloat16)
    normed_cols = lax.dynamic_slice_in_dim(normed, lax.axis_index("tp") * col_width, col_width, 1)
    flat_expert = expert_ids.reshape(-1)
    one_hot = (flat_expert[:, None] == jnp.arange(experts, dtype=jnp.int32)[None, :]).astype(
        jnp.int32
    )
    running = jnp.cumsum(one_hot, axis=0)
    rank = jnp.sum((running - one_hot) * one_hot, axis=1)
    dest = flat_expert * capacity + rank
    token_of = jnp.arange(tok_rows * top_count, dtype=jnp.int32) // top_count
    slot_token = jnp.full((experts * capacity,), tok_rows, jnp.int32).at[dest].set(token_of)
    padded = jnp.concatenate([normed_cols, jnp.zeros((1, col_width), jnp.bfloat16)], axis=0)
    outgoing = padded[slot_token].reshape(group_count, shard_count, capacity, col_width)
    arrived = lax.all_to_all(outgoing, "fs", split_axis=1, concat_axis=1, tiled=True)
    slot_rows = arrived.reshape(group_count, shard_count * capacity, col_width)
    pair_weight = jnp.stack([new_gate[:, 0], new_up[:, 0]], axis=2).reshape(
        group_count, 2 * hidden, col_width
    )
    rows_weight = pair_weight
    term = jnp.einsum("ihd,ird->hir", rows_weight, slot_rows, preferred_element_type=jnp.float32)
    pair_sum = lax.psum_scatter(
        term.reshape(
            2 * hidden // column_count * lax.axis_size("tp"), group_count * shard_count * capacity
        ).astype(jnp.bfloat16),
        "tp",
        scatter_dimension=0,
        tiled=True,
    ).astype(jnp.float32)
    pair_sum = pair_sum.reshape(hidden // column_count, 2, group_count, shard_count * capacity)
    activation = (jax.nn.silu(pair_sum[:, 0]) * pair_sum[:, 1]).astype(jnp.bfloat16)
    down_local = new_down[:, 0]
    rows_down = down_local
    slot_out = jnp.einsum(
        "hir,ihd->ird",
        lax.all_gather(activation, "tp", axis=0, tiled=True),
        rows_down,
        preferred_element_type=jnp.float32,
    )
    returning = slot_out.astype(jnp.bfloat16).reshape(group_count, shard_count, capacity, col_width)
    returned = lax.all_to_all(returning, "fs", split_axis=1, concat_axis=1, tiled=True)
    result_rows = returned.reshape(experts * capacity, col_width)
    picked = result_rows[dest].reshape(tok_rows, top_count, col_width).astype(jnp.float32)
    share = route_weight / jnp.sum(route_weight, axis=1, keepdims=True) * route_scale
    routed = jnp.sum(share[:, :, None] * picked, axis=1)
    shared_pair = jnp.stack([new_shared_gate, new_shared_up], axis=1).reshape(
        2 * shared_hidden, col_width
    )
    rows_weight = shared_pair
    shared_sum = lax.psum_scatter(
        lax.dot_general(
            rows_weight, normed_cols, (((1,), (1,)), ((), ())), preferred_element_type=jnp.float32
        ).astype(jnp.bfloat16),
        "tp",
        scatter_dimension=0,
        tiled=True,
    ).astype(jnp.float32)
    shared_sum = shared_sum.reshape(shared_hidden // column_count, 2, tok_rows)
    shared_act = (jax.nn.silu(shared_sum[:, 0]) * shared_sum[:, 1]).astype(jnp.bfloat16)
    rows_down = new_shared_down
    shared_out = lax.dot_general(
        lax.all_gather(shared_act, "tp", axis=0, tiled=True),
        rows_down,
        (((0,), (0,)), ((), ())),
        preferred_element_type=jnp.float32,
    )
    mixed = (shared_out + routed).astype(jnp.bfloat16)
    return (mixed, new_gate, new_up, new_down, new_shared_gate, new_shared_up, new_shared_down)


def solution(mesh):
    placed = (
        P(("gr", "fs"), None),
        P(("gr", "fs"), None),
        P(("gr", "fs"), None),
        P("tp"),
        P("gr", "fs", "tp"),
        P("gr", "fs", "tp"),
        P("gr", "fs", "tp"),
        P("fs", "tp"),
        P("fs", "tp"),
        P("fs", "tp"),
    )
    return jax.shard_map(
        body,
        mesh=mesh,
        in_specs=placed,
        out_specs=(
            P(("gr", "fs"), "tp"),
            P(None, "fs", None, "tp"),
            P(None, "fs", None, "tp"),
            P(None, "fs", None, "tp"),
            P(None, "tp"),
            P(None, "tp"),
            P(None, "tp"),
        ),
        check_vma=False,
    )
```

profile of v0, /device:TPU:0, one launch (start us, length us, event | category | flops | bytes accessed | tf_op | source)
XLA Modules:
  0.0 498.0 jit_solution(3929009726196123222)
XLA Ops:
  7.2 4.0 multiply_convert_fusion.1
  11.2 7.4 %all-to-all-start.2 = ((bf16[8,64,1024]{2,1,0:T(8,128)(2,1)}), bf16[8,64,1024]{2,1,0:T(8,128)(2,1)S(1)}, u32[]{:S(2)}, u32[]{:S(2)}) async-start(bf16[8,64,1024]{2,1,0:T(8,128)(2,1)} %get-tuple-element.42), calls=%async_computation.3 | async-start | bytes 2097152 | tf_op jit(solution)/shard_map/all_to_all | solution.py:41
  19.0 1.3 convert_element_type.65
  20.5 23.9 %all-to-all-done.2 = bf16[8,64,1024]{2,1,0:T(8,128)(2,1)S(1)} async-done(((bf16[8,64,1024]{2,1,0:T(8,128)(2,1)}), bf16[8,64,1024]{2,1,0:T(8,128)(2,1)S(1)}, u32[]{:S(2)}, u32[]{:S(2)}) %all-to-all-start.2) | async-done | bytes 1048608 | tf_op jit(solution)/shard_map/all_to_all | solution.py:41
  44.4 3.6 all-to-all-start.1
  48.0 4.5 reduce-window.6
  52.6 0.4 slice_reduce_fusion
  53.4 1.2 fusion.11
  54.9 7.6 %scatter_custom_fusion = s32[1760]{0:T(1024)S(1)} fusion(s32[1408]{0:T(1024)S(1)} %fusion.23, s32[1408]{0:T(1024)S(1)} %add_select_fusion, s32[]{:T(128)} %constant.49.clone.1), kind=kCustom, calls=%fused_computation.58 | custom fusion | bytes 7044 | tf_op jit(solution)/shard_map/scatter | solution.py:70
  62.5 6.6 %gather_fusion = bf16[1760,1024]{1,0:T(8,128)(2,1)} fusion(bf16[177,1024]{1,0:T(8,128)(2,1)S(1)} %concatenate.3, s32[2048]{0:T(1024)S(1)} %pad_clamp_fusion.1), kind=kCustom, calls=%fused_computation | custom fusion | bytes 7216000 | tf_op jit(solution)/shard_map/gather | solution.py:72
  69.1 4.8 reshape.129
  73.8 7.6 %copy.55 = bf16[2,8,110,1024]{3,0,2,1:T(2,128)(2,1)} copy(bf16[2,8,110,1024]{3,2,1,0:T(8,128)(2,1)} %reshape.129) | data formatting | bytes 7208960 | tf_op jit(solution)/shard_map/reshape | solution.py:72
  81.4 1.0 copy-done.4
  82.4 6.0 %all-to-all-start = ((bf16[2,8,110,1024]{3,0,2,1:T(2,128)(2,1)}), bf16[2,8,110,1024]{3,0,2,1:T(2,128)(2,1)}, u32[]{:S(2)}, u32[]{:S(2)}) async-start(bf16[2,8,110,1024]{3,0,2,1:T(2,128)(2,1)} %copy.55), calls=%async_computation.1 | async-start | bytes 7208960 | tf_op jit(solution)/shard_map/all_to_all | solution.py:73
  88.4 0.7 all-gather.16.cloned.1.call-update
  89.1 0.7 all-gather.14.cloned.1.call-update
  89.8 0.5 reduce-scatter.5.cloned.1.call-start
  90.4 35.5 %all-gather.16.cloned.1.call-done = bf16[2,512,1024]{2,1,0:T(8,128)(2,1)} async-done(((bf16[1,512,1024]{2,1,0:T(8,128)(2,1)}), bf16[2,512,1024]{2,1,0:T(8,128)(2,1)}) %all-gather.16.cloned.1.call-update) | async-done | bytes 2097168 | tf_op jit(solution)/shard_map/all_gather | solution.py:46
  125.8 35.2 %all-gather.14.cloned.1.call-done = bf16[2,512,1024]{2,1,0:T(8,128)(2,1)} async-done(((bf16[1,512,1024]{2,1,0:T(8,128)(2,1)}), bf16[2,512,1024]{2,1,0:T(8,128)(2,1)}) %all-gather.14.cloned.1.call-update) | async-done | bytes 2097168 | tf_op jit(solution)/shard_map/all_gather | solution.py:45
  161.1 2.6 pad_maximum_fusion
  163.7 6.3 %copy.57 = bf16[2,512,2,1024]{3,2,1,0:T(2,128)(2,1)} copy(bf16[2,512,2,1024]{3,1,0,2:T(8,128)(2,1)S(1)} %pad_maximum_fusion) | data formatting | bytes 8388608 | tf_op jit(solution)/shard_map/stack | solution.py:75
  170.0 7.2 %reshape.131 = bf16[2,1024,1024]{2,1,0:T(8,128)(2,1)} reshape(bf16[2,512,2,1024]{3,2,1,0:T(2,128)(2,1)} %copy.57) | data formatting | bytes 8388608 | tf_op jit(solution)/shard_map/reshape | solution.py:75
  177.2 9.0 %fusion.3 = bf16[2,880,1024]{2,1,0:T(8,128)(2,1)} fusion(bf16[2,1024,1024]{2,1,0:T(8,128)(2,1)} %reshape.131, bf16[2,880,1024]{2,0,1:T(2,128)(2,1)} %bitcast.5), kind=kOutput, calls=%fused_computation.8 | convolution fusion | flops 3692789760 | bytes 11403264 | tf_op jit(solution)/shard_map/ihd,ird->hir/dot_general | solution.py:79
  186.2 5.8 %copy.58 = bf16[1024,1760]{1,0:T(8,128)(2,1)} copy(bf16[1024,1760]{0,1:T(8,128)(2,1)} %bitcast.93) | data formatting | bytes 7208960 | tf_op jit(solution)/shard_map/convert_element_type | solution.py:83
  192.1 1.5 copy-done.8
  193.7 31.0 %all_to_all.46 = bf16[8,64,1024]{2,1,0:T(8,128)(2,1)} all-to-all(bf16[8,64,1024]{2,1,0:T(8,128)(2,1)S(1)} %convert_element_type.78), channel_id=1, replica_groups=mesh['gr'=2,'fs'=8,'tp'=2] {'fs'}, dimensions={0} | all-to-all | bytes 2097152 | tf_op jit(solution)/shard_map/all_to_all | solution.py:42
  225.0 5.6 %reshape.142 = f32[256,2,2,880]{3,2,1,0:T(2,128)} reshape(bf16[512,1760]{1,0:T(8,128)(2,1)} %reduce-scatter.5.cloned.1.call-done) | data formatting | bytes 5406720 | tf_op jit(solution)/shard_map/reshape | solution.py:88
  230.6 4.8 fusion.26
  235.4 3.9 copy.69
  239.3 2.5 copy.68
  241.9 3.5 fusion.6
  245.5 0.7 multiply_convert_fusion.3
  246.2 9.9 %all-gather.20.cloned.1.call-done = bf16[2,512,1024]{2,1,0:T(8,128)(2,1)} async-done(((bf16[1,512,1024]{2,1,0:T(8,128)(2,1)}), bf16[2,512,1024]{2,1,0:T(8,128)(2,1)}) %all-gather.20.cloned.1.call-update) | async-done | bytes 2097168 | tf_op jit(solution)/shard_map/all_gather | solution.py:47
  256.1 11.7 %all-gather.18.cloned.1.call-done = bf16[512,2,880]{0,2,1:T(8,128)(2,1)} async-done(((bf16[256,2,880]{0,2,1:T(8,128)(2,1)}), bf16[512,2,880]{0,2,1:T(8,128)(2,1)}) %all-gather.18.cloned.1.call-update) | async-done | bytes 1802256 | tf_op jit(solution)/shard_map/all_gather | solution.py:94
  267.8 4.2 convolution_convert_fusion
  272.0 5.5 %copy.67 = bf16[2,880,1024]{2,0,1:T(2,128)(2,1)} copy(bf16[2,880,1024]{2,1,0:T(8,128)(2,1)S(1)} %convolution_convert_fusion) | data formatting | bytes 7208960 | tf_op jit(solution)/shard_map/reshape | solution.py:98
  277.5 5.9 %all-to-all-start.4 = ((bf16[2,8,110,1024]{3,0,2,1:T(2,128)(2,1)}), bf16[2,8,110,1024]{3,0,2,1:T(2,128)(2,1)}, u32[]{:S(2)}, u32[]{:S(2)}) async-start(bf16[2,8,110,1024]{3,0,2,1:T(2,128)(2,1)} %bitcast.83), calls=%async_computation.6 | async-start | bytes 7208960 | tf_op jit(solution)/shard_map/all_to_all | solution.py:99
  283.5 0.7 all-gather.8.cloned.1.call-update
  284.2 0.7 convert_element_type.69
  285.2 75.8 %all-gather.10.cloned.1.call-done = bf16[512,1024]{1,0:T(8,128)(2,1)} async-done(((bf16[64,1024]{1,0:T(8,128)(2,1)}), bf16[512,1024]{1,0:T(8,128)(2,1)}) %all-gather.10.cloned.1.call-update) | async-done | bytes 1048592 | tf_op jit(solution)/shard_map/all_gather | solution.py:54
  361.0 42.5 %all-gather.8.cloned.1.call-done = bf16[512,1024]{1,0:T(8,128)(2,1)} async-done(((bf16[64,1024]{1,0:T(8,128)(2,1)}), bf16[512,1024]{1,0:T(8,128)(2,1)}) %all-gather.8.cloned.1.call-update) | async-done | bytes 1048592 | tf_op jit(solution)/shard_map/all_gather | solution.py:53
  403.5 1.7 pad_maximum_fusion.1
  405.3 2.2 copy.47
  407.4 2.2 reshape.125
  409.6 3.2 convolution_convert_fusion.1
  413.0 32.2 %all-gather.12.cloned.1.call-done = bf16[512,1024]{1,0:T(8,128)(2,1)} async-done(((bf16[64,1024]{1,0:T(8,128)(2,1)}), bf16[512,1024]{1,0:T(8,128)(2,1)}) %all-gather.12.cloned.1.call-update) | async-done | bytes 1048592 | tf_op jit(solution)/shard_map/all_gather | solution.py:55
  445.3 9.4 %reduce-scatter.3.cloned.1.call-done = bf16[512,176]{0,1:T(8,128)(2,1)} async-done(((bf16[1024,176]{0,1:T(8,128)(2,1)}), bf16[512,176]{0,1:T(8,128)(2,1)}) %reduce-scatter.3.cloned.1.call-update) | async-done | bytes 180240 | tf_op jit(solution)/shard_map/reduce_scatter | solution.py:108
  454.6 1.1 copy.48
  456.7 1.9 all_gather.26
  458.7 5.0 copy.62
  463.6 4.8 reshape.135
  468.4 9.7 %gather_fusion.1 = bf16[1408,1024]{1,0:T(8,128)(2,1)S(1)} fusion(bf16[1760,1024]{1,0:T(8,128)(2,1)} %reshape.135, s32[2048]{0:T(1024)S(1)} %pad_clamp_fusion), kind=kCustom, calls=%fused_computation.1 | custom fusion | bytes 5772800 | tf_op jit(solution)/shard_map/gather | solution.py:101
  478.2 1.7 fusion
  479.9 1.1 fusion.10
  481.0 1.3 copy.82
  482.3 1.0 copy-done
  483.4 1.3 copy.83
  484.7 1.0 copy-done.9
  485.7 1.3 copy.84
  487.0 0.6 copy-done.6
  487.7 1.0 copy.85
  488.6 0.6 copy-done.5
  489.3 1.0 copy.86
  490.2 1.0 copy.87
  (71 shorter events, 3.3 us)
Async XLA Ops:
  11.2 7.4 %copy-start.13 = (s32[176,8]{0,1:T(8,128)S(1)}, s32[176,8]{0,1:T(8,128)}, u32[]{:S(2)}) copy-start(s32[176,8]{0,1:T(8,128)} %param.11) | copy-start | bytes 16900
  11.2 7.8 %copy-start.7 = (bf16[176,2048]{1,0:T(8,128)(2,1)S(1)}, bf16[176,2048]{1,0:T(8,128)(2,1)}, u32[]{:S(2)}) copy-start(bf16[176,2048]{1,0:T(8,128)(2,1)} %param.10) | copy-start | bytes 2162692
  11.2 33.2 %all-to-all-start.2 = ((bf16[8,64,1024]{2,1,0:T(8,128)(2,1)}), bf16[8,64,1024]{2,1,0:T(8,128)(2,1)S(1)}, u32[]{:S(2)}, u32[]{:S(2)}) async-start(bf16[8,64,1024]{2,1,0:T(8,128)(2,1)} %get-tuple-element.42), calls=%async_computation.3 | async-start | bytes 2097152 | tf_op jit(solution)/shard_map/all_to_all | solution.py:41
  44.4 10.2 %copy-start.2 = (bf16[8,64,1024]{2,1,0:T(8,128)(2,1)}, bf16[8,64,1024]{2,1,0:T(8,128)(2,1)S(1)}, u32[]{:S(2)}) copy-start(bf16[8,64,1024]{2,1,0:T(8,128)(2,1)S(1)} %all-to-all-done.2) | copy-start | bytes 3145732
  44.4 37.0 %all-to-all-start.1 = ((bf16[8,64,1024]{2,1,0:T(8,128)(2,1)}), bf16[8,64,1024]{2,1,0:T(8,128)(2,1)S(1)}, u32[]{:S(2)}, u32[]{:S(2)}) async-start(bf16[8,64,1024]{2,1,0:T(8,128)(2,1)} %get-tuple-element.41), calls=%async_computation.2 | async-start | bytes 2097152 | tf_op jit(solution)/shard_map/all_to_all | solution.py:40
  81.4 1.0 copy-start.4
  82.4 94.8 %all-to-all-start = ((bf16[2,8,110,1024]{3,0,2,1:T(2,128)(2,1)}), bf16[2,8,110,1024]{3,0,2,1:T(2,128)(2,1)}, u32[]{:S(2)}, u32[]{:S(2)}) async-start(bf16[2,8,110,1024]{3,0,2,1:T(2,128)(2,1)} %copy.55), calls=%async_computation.1 | async-start | bytes 7208960 | tf_op jit(solution)/shard_map/all_to_all | solution.py:73
  88.4 37.4 %all-gather.16.cloned.1.call-start = ((), (), s32[]{:S(2)}) async-start(), calls=%async_computation.12 | async-start | bytes 3145728 | tf_op jit(solution)/shard_map/all_gather | solution.py:46
  89.1 72.0 %all-gather.14.cloned.1.call-start = ((), (), s32[]{:S(2)}) async-start(), calls=%async_computation.11 | async-start | bytes 3145728 | tf_op jit(solution)/shard_map/all_gather | solution.py:45
  89.8 135.2 %reduce-scatter.5.cloned.1.call-start = ((), (), s32[]{:S(2)}) async-start(), calls=%async_computation.13 | async-start | bytes 5505024 | tf_op jit(solution)/shard_map/reduce_scatter | solution.py:80
  192.0 1.6 copy-start.8
  192.0 64.1 %all-gather.20.cloned.1.call-start = ((), (), s32[]{:S(2)}) async-start(), calls=%async_computation.15 | async-start | bytes 3145728 | tf_op jit(solution)/shard_map/all_gather | solution.py:47
  224.8 43.1 %all-gather.18.cloned.1.call-start = ((), (), s32[]{:S(2)}) async-start(), calls=%async_computation.14 | async-start | bytes 2703360 | tf_op jit(solution)/shard_map/all_gather | solution.py:94
  241.8 3.6 copy-start.10
  241.9 3.6 copy-start.11
  241.9 3.6 copy-start.15
  245.4 115.6 %all-gather.10.cloned.1.call-start = ((), (), s32[]{:S(2)}) async-start(), calls=%async_computation.8 | async-start | bytes 1179648 | tf_op jit(solution)/shard_map/all_gather | solution.py:54
  277.5 6.7 %copy-start.12 = (f32[64,1024]{1,0:T(8,128)S(1)}, f32[64,1024]{1,0:T(8,128)}, u32[]{:S(2)}) copy-start(f32[64,1024]{1,0:T(8,128)} %param.19) | copy-start | bytes 786436
  277.5 181.2 %all-to-all-start.4 = ((bf16[2,8,110,1024]{3,0,2,1:T(2,128)(2,1)}), bf16[2,8,110,1024]{3,0,2,1:T(2,128)(2,1)}, u32[]{:S(2)}, u32[]{:S(2)}) async-start(bf16[2,8,110,1024]{3,0,2,1:T(2,128)(2,1)} %bitcast.83), calls=%async_computation.6 | async-start | bytes 7208960 | tf_op jit(solution)/shard_map/all_to_all | solution.py:99
  283.4 120.1 %all-gather.8.cloned.1.call-start = ((), (), s32[]{:S(2)}) async-start(), calls=%async_computation.7 | async-start | bytes 1179648 | tf_op jit(solution)/shard_map/all_gather | solution.py:53
  284.2 161.1 %all-gather.12.cloned.1.call-start = ((), (), s32[]{:S(2)}) async-start(), calls=%async_computation.10 | async-start | bytes 1179648 | tf_op jit(solution)/shard_map/all_gather | solution.py:55
  284.9 169.7 %reduce-scatter.3.cloned.1.call-start = ((), (), s32[]{:S(2)}) async-start(), calls=%async_computation.9 | async-start | bytes 540672 | tf_op jit(solution)/shard_map/reduce_scatter | solution.py:108
  409.6 3.2 copy-start.14
  478.1 1.8 copy-start.3
  478.1 2.9 copy-start.1
  481.0 2.3 copy-start
  483.4 2.3 copy-start.9
  485.7 2.0 copy-start.6
  487.7 1.6 copy-start.5
Sparse Core Ops, SparseCore 0:
  91.3 34.4 all-gather.15
  127.9 33.0 all-gather.13
  192.1 11.8 reduce-scatter.4
  224.9 31.1 all-gather.19
  258.1 9.7 all-gather.17
  270.4 90.5 all-gather.9
  363.7 39.7 all-gather.7
  406.2 38.9 all-gather.11
  448.1 6.5 reduce-scatter.2
where the time goes:
time: 506 us; the launch traced here: 498 us
  waiting for transfers between devices  278 us (55%)
  local copies, waits for them, and re-layouts  108 us (21%)
  blocking collectives  33 us (7%)
  starting transfers between devices  24.2 us (5%)
  other arithmetic  22.9 us (5%)
  matrix products  17.4 us (3%)
  between operations  14.4 us (3%)
    all_gather x1, waiting for transfers between devices, body(): lax.all_gather(fold_gain(shared_up, norm_gain), 'fs', axis=0, tiled=True)  75.8 us
    all_gather x1, waiting for transfers between devices, body(): lax.all_gather(fold_gain(shared_gate, norm_gain), 'fs', axis=0, tiled=True)  42.5 us
    all_gather x1, waiting for transfers between devices, body(): lax.all_gather(moved[1], 'gr', axis=0, tiled=True)  35.5 us
    all_gather x1, waiting for transfers between devices, body(): lax.all_gather(moved[0], 'gr', axis=0, tiled=True)  35.2 us
    all_gather x1, waiting for transfers between devices, body(): lax.all_gather(shared_down.astype(jnp.bfloat16), 'fs', axis=0, tiled=True)  32.2 us
    all_to_all x1, blocking collectives, body(): lax.all_to_all(down_round, 'fs', split_axis=0, concat_axis=1, tiled=True)  31 us
    all_to_all x1, waiting for transfers between devices, body(): lax.all_to_all(up_round, 'fs', split_axis=0, concat_axis=1, tiled=True)  23.9 us
    unnamed x41, local copies, waits for them, and re-layouts  19.3 us
  transfers between devices with their start and end apart: 13, of which 9 were waited for; matrix products, arithmetic and copies ran while one was open for 19% of the time, Pallas kernels for 0%

commit v1 on v0

--- a/solution.py
+++ b/solution.py
@@ -42,7 +42,11 @@
         lax.all_to_all(down_round, "fs", split_axis=0, concat_axis=1, tiled=True),
     )
     whole = (
-        lax.all_gather(moved[0], "gr", axis=0, tiled=True),
+        jnp.roll(
+            jnp.concatenate([moved[0], lax.ppermute(moved[0], "gr", [(0, 1), (1, 0)])], axis=0),
+            lax.axis_index("gr") * moved[0].shape[0],
+            axis=0,
+        ),
         lax.all_gather(moved[1], "gr", axis=0, tiled=True),
         lax.all_gather(moved[2], "gr", axis=0, tiled=True),
     )

time: 506 us -> 495 us (0.978)
  waiting for transfers between devices: 278 us -> 257 us
  other arithmetic: 22.9 us -> 30 us
    ppermute x0 -> x1, waiting for transfers between devices: none -> 35.5 us  [body(): lax.ppermute(moved[0], 'gr', [(0, 1), (1, 0)])]
    all_gather x1 -> x0, waiting for transfers between devices: 35.2 us -> none  [body(): lax.all_gather(moved[0], 'gr', axis=0, tiled=True)]
    all_gather x1, waiting for transfers between devices: 42.5 us -> 76 us  [body(): lax.all_gather(fold_gain(shared_gate, norm_gain), 'fs', axis=0, tiled=True)]
    all_gather x1, waiting for transfers between devices: 75.8 us -> 42.6 us  [body(): lax.all_gather(fold_gain(shared_up, norm_gain), 'fs', axis=0, tiled=True)]
    all_gather x1, waiting for transfers between devices: 35.5 us -> 7.21 us  [body(): lax.all_gather(moved[1], 'gr', axis=0, tiled=True)]
    all_to_all x1, waiting for transfers between devices: 23.9 us -> 0.01 us  [body(): lax.all_to_all(up_round, 'fs', split_axis=0, concat_axis=1, tiled=True)]
    all_to_all x1, waiting for transfers between devices: 0.01 us -> 19.6 us  [body(): lax.all_to_all(gate_round, 'fs', split_axis=0, concat_axis=1, tiled=True)]
    all_to_all x1, waiting for transfers between devices: 0.01 us -> 15.9 us  [body(): lax.all_to_all(outgoing, 'fs', split_axis=1, concat_axis=1, tiled=True)]
  transfers between devices with their start and end apart: 13 -> 13, of which waited for: 9 -> 10; matrix products, arithmetic and copies ran while one was open for 19% -> 22% of each run, Pallas kernels for 0% -> 0%
where the time goes in v1:
time: 495 us; the launch traced here: 487 us
  waiting for transfers between devices  257 us (52%)
  local copies, waits for them, and re-layouts  111 us (22%)
  blocking collectives  31.4 us (6%)
  other arithmetic  30 us (6%)
  starting transfers between devices  25.7 us (5%)
  matrix products  17.5 us (4%)
  between operations  14.7 us (3%)
    all_gather x1, waiting for transfers between devices, body(): lax.all_gather(fold_gain(shared_gate, norm_gain), 'fs', axis=0, tiled=True)  76 us
    all_gather x1, waiting for transfers between devices, body(): lax.all_gather(fold_gain(shared_up, norm_gain), 'fs', axis=0, tiled=True)  42.6 us
    ppermute x1, waiting for transfers between devices, body(): lax.ppermute(moved[0], 'gr', [(0, 1), (1, 0)])  35.5 us
    all_to_all x1, blocking collectives, body(): lax.all_to_all(down_round, 'fs', split_axis=0, concat_axis=1, tiled=True)  29.4 us
    all_gather x1, waiting for transfers between devices, body(): lax.all_gather(shared_down.astype(jnp.bfloat16), 'fs', axis=0, tiled=True)  29 us
    all_to_all x1, waiting for transfers between devices, body(): lax.all_to_all(gate_round, 'fs', split_axis=0, concat_axis=1, tiled=True)  19.6 us
    unnamed x34, local copies, waits for them, and re-layouts  16.8 us
    all_to_all x1, waiting for transfers between devices, body(): lax.all_to_all(outgoing, 'fs', split_axis=1, concat_axis=1, tiled=True)  15.9 us
  transfers between devices with their start and end apart: 13, of which 10 were waited for; matrix products, arithmetic and copies ran while one was open for 22% of the time, Pallas kernels for 0%

profile of v1, /device:TPU:0, one launch (start us, length us, event | category | flops | bytes accessed | tf_op | source)
XLA Modules:
  0.0 487.2 jit_solution(3675516538545732308)
XLA Ops:
  7.2 4.0 multiply_convert_fusion.1
  11.2 7.4 %all-to-all-start.1 = ((bf16[8,64,1024]{2,1,0:T(8,128)(2,1)}), bf16[8,64,1024]{2,1,0:T(8,128)(2,1)S(1)}, u32[]{:S(2)}, u32[]{:S(2)}) async-start(bf16[8,64,1024]{2,1,0:T(8,128)(2,1)} %get-tuple-element.41), calls=%async_computation.2 | async-start | bytes 2097152 | tf_op jit(solution)/shard_map/all_to_all | solution.py:40
  19.0 1.3 convert_element_type.65
  20.3 4.5 reduce-window.6
  24.8 19.6 %all-to-all-done.1 = bf16[8,64,1024]{2,1,0:T(8,128)(2,1)S(1)} async-done(((bf16[8,64,1024]{2,1,0:T(8,128)(2,1)}), bf16[8,64,1024]{2,1,0:T(8,128)(2,1)S(1)}, u32[]{:S(2)}, u32[]{:S(2)}) %all-to-all-start.1) | async-done | bytes 1048608 | tf_op jit(solution)/shard_map/all_to_all | solution.py:40
  44.4 3.6 all-to-all-start.2
  49.1 1.2 fusion.14
  50.5 7.6 %scatter_custom_fusion = s32[1760]{0:T(1024)S(1)} fusion(s32[1408]{0:T(1024)S(1)} %fusion.26, s32[1408]{0:T(1024)S(1)} %add_select_fusion, s32[]{:T(128)} %constant.70.clone.1), kind=kCustom, calls=%fused_computation.65 | custom fusion | bytes 7044 | tf_op jit(solution)/shard_map/scatter | solution.py:74
  58.2 6.6 %gather_fusion = bf16[1760,1024]{1,0:T(8,128)(2,1)} fusion(bf16[177,1024]{1,0:T(8,128)(2,1)S(1)} %concatenate.9, s32[2048]{0:T(1024)S(1)} %pad_clamp_fusion.1), kind=kCustom, calls=%fused_computation | custom fusion | bytes 7216000 | tf_op jit(solution)/shard_map/gather | solution.py:76
  64.8 4.8 reshape.129
  69.5 7.6 %copy.55 = bf16[2,8,110,1024]{3,0,2,1:T(2,128)(2,1)} copy(bf16[2,8,110,1024]{3,2,1,0:T(8,128)(2,1)} %reshape.129) | data formatting | bytes 7208960 | tf_op jit(solution)/shard_map/reshape | solution.py:76
  77.1 1.0 copy-done.1
  78.1 6.0 %all-to-all-start = ((bf16[2,8,110,1024]{3,0,2,1:T(2,128)(2,1)}), bf16[2,8,110,1024]{3,0,2,1:T(2,128)(2,1)}, u32[]{:S(2)}, u32[]{:S(2)}) async-start(bf16[2,8,110,1024]{3,0,2,1:T(2,128)(2,1)} %copy.55), calls=%async_computation.1 | async-start | bytes 7208960 | tf_op jit(solution)/shard_map/all_to_all | solution.py:77
  84.1 0.7 all-gather.13.cloned.1.call-update
  85.3 1.6 collective-permute-start
  86.9 35.5 %collective-permute-done = bf16[1,512,1024]{2,1,0:T(8,128)(2,1)S(1)} collective-permute-done((bf16[1,512,1024]{2,1,0:T(8,128)(2,1)S(1)}, bf16[1,512,1024]{2,1,0:T(8,128)(2,1)S(1)}, u32[]{:S(2)}, u32[]{:S(2)}) %collective-permute-start) | collective-permute-done | bytes 1048608 | tf_op jit(solution)/shard_map/ppermute | solution.py:46
  122.4 2.8 fusion.39
  125.1 7.2 %all-gather.13.cloned.1.call-done = bf16[2,512,1024]{2,1,0:T(8,128)(2,1)} async-done(((bf16[1,512,1024]{2,1,0:T(8,128)(2,1)}), bf16[2,512,1024]{2,1,0:T(8,128)(2,1)}) %all-gather.13.cloned.1.call-update) | async-done | bytes 2097168 | tf_op jit(solution)/shard_map/all_gather | solution.py:50
  132.3 2.6 pad_maximum_fusion
  134.9 6.3 %copy.57 = bf16[2,512,2,1024]{3,2,1,0:T(2,128)(2,1)} copy(bf16[2,512,2,1024]{3,1,0,2:T(8,128)(2,1)S(1)} %pad_maximum_fusion) | data formatting | bytes 8388608 | tf_op jit(solution)/shard_map/stack | solution.py:79
  141.2 7.2 %reshape.131 = bf16[2,1024,1024]{2,1,0:T(8,128)(2,1)} reshape(bf16[2,512,2,1024]{3,2,1,0:T(2,128)(2,1)} %copy.57) | data formatting | bytes 8388608 | tf_op jit(solution)/shard_map/reshape | solution.py:79
  148.4 15.9 %all-to-all-done = bf16[2,8,110,1024]{3,0,2,1:T(2,128)(2,1)} async-done(((bf16[2,8,110,1024]{3,0,2,1:T(2,128)(2,1)}), bf16[2,8,110,1024]{3,0,2,1:T(2,128)(2,1)}, u32[]{:S(2)}, u32[]{:S(2)}) %all-to-all-start) | async-done | bytes 3604512 | tf_op jit(solution)/shard_map/all_to_all | solution.py:77
  164.3 9.0 %fusion.3 = bf16[2,880,1024]{2,1,0:T(8,128)(2,1)} fusion(bf16[2,1024,1024]{2,1,0:T(8,128)(2,1)} %reshape.131, bf16[2,880,1024]{2,0,1:T(2,128)(2,1)} %bitcast.5), kind=kOutput, calls=%fused_computation.12 | convolution fusion | flops 3692789760 | bytes 11403264 | tf_op jit(solution)/shard_map/ihd,ird->hir/dot_general | solution.py:83
  173.3 5.9 %copy.58 = bf16[1024,1760]{1,0:T(8,128)(2,1)} copy(bf16[1024,1760]{0,1:T(8,128)(2,1)} %bitcast.93) | data formatting | bytes 7208960 | tf_op jit(solution)/shard_map/convert_element_type | solution.py:87
  179.2 1.7 convert_element_type.78
  181.0 29.4 %all_to_all.46 = bf16[8,64,1024]{2,1,0:T(8,128)(2,1)} all-to-all(bf16[8,64,1024]{2,1,0:T(8,128)(2,1)S(1)} %convert_element_type.78), channel_id=1, replica_groups=mesh['gr'=2,'fs'=8,'tp'=2] {'fs'}, dimensions={0} | all-to-all | bytes 2097152 | tf_op jit(solution)/shard_map/all_to_all | solution.py:42
  210.7 5.6 %reshape.142 = f32[256,2,2,880]{3,2,1,0:T(2,128)} reshape(bf16[512,1760]{1,0:T(8,128)(2,1)} %reduce-scatter.5.cloned.1.call-done) | data formatting | bytes 5406720 | tf_op jit(solution)/shard_map/reshape | solution.py:92
  216.3 5.4 %fusion.29 = (f32[256,1,2,880]{3,2,1,0:T(2,128)}, f32[256,1,2,880]{3,2,1,0:T(2,128)}) fusion(f32[256,2,2,880]{3,2,1,0:T(2,128)} %reshape.142), kind=kLoop, calls=%fused_computation.68 | loop fusion | bytes 7208960 | tf_op jit(solution)/shard_map/slice | solution.py:93
  221.7 3.9 copy.67
  225.6 3.9 copy.68
  229.6 3.5 fusion.9
  233.2 0.7 multiply_convert_fusion.3
  233.9 8.8 %all-gather.17.cloned.1.call-done = bf16[2,512,1024]{2,1,0:T(8,128)(2,1)} async-done(((bf16[1,512,1024]{2,1,0:T(8,128)(2,1)}), bf16[2,512,1024]{2,1,0:T(8,128)(2,1)}) %all-gather.17.cloned.1.call-update) | async-done | bytes 2097168 | tf_op jit(solution)/shard_map/all_gather | solution.py:51
  242.8 11.7 %all-gather.15.cloned.1.call-done = bf16[512,2,880]{0,2,1:T(8,128)(2,1)} async-done(((bf16[256,2,880]{0,2,1:T(8,128)(2,1)}), bf16[512,2,880]{0,2,1:T(8,128)(2,1)}) %all-gather.15.cloned.1.call-update) | async-done | bytes 1802256 | tf_op jit(solution)/shard_map/all_gather | solution.py:98
  254.5 4.2 convolution_convert_fusion
  258.7 5.5 %copy.66 = bf16[2,880,1024]{2,0,1:T(2,128)(2,1)} copy(bf16[2,880,1024]{2,1,0:T(8,128)(2,1)S(1)} %convolution_convert_fusion) | data formatting | bytes 7208960 | tf_op jit(solution)/shard_map/reshape | solution.py:102
  264.2 5.9 %all-to-all-start.4 = ((bf16[2,8,110,1024]{3,0,2,1:T(2,128)(2,1)}), bf16[2,8,110,1024]{3,0,2,1:T(2,128)(2,1)}, u32[]{:S(2)}, u32[]{:S(2)}) async-start(bf16[2,8,110,1024]{3,0,2,1:T(2,128)(2,1)} %bitcast.83), calls=%async_computation.6 | async-start | bytes 7208960 | tf_op jit(solution)/shard_map/all_to_all | solution.py:103
  270.1 0.5 all-gather.9.cloned.1.call-update
  270.7 0.7 convert_element_type.69
  271.7 76.0 %all-gather.7.cloned.1.call-done = bf16[512,1024]{1,0:T(8,128)(2,1)} async-done(((bf16[64,1024]{1,0:T(8,128)(2,1)}), bf16[512,1024]{1,0:T(8,128)(2,1)}) %all-gather.7.cloned.1.call-update) | async-done | bytes 1048592 | tf_op jit(solution)/shard_map/all_gather | solution.py:57
  347.6 42.6 %all-gather.9.cloned.1.call-done = bf16[512,1024]{1,0:T(8,128)(2,1)} async-done(((bf16[64,1024]{1,0:T(8,128)(2,1)}), bf16[512,1024]{1,0:T(8,128)(2,1)}) %all-gather.9.cloned.1.call-update) | async-done | bytes 1048592 | tf_op jit(solution)/shard_map/all_gather | solution.py:58
  390.2 1.7 pad_maximum_fusion.1
  392.0 3.5 copy.47
  395.4 4.1 reshape.125
  399.5 3.2 convolution_convert_fusion.1
  403.0 29.0 %all-gather.11.cloned.1.call-done = bf16[512,1024]{1,0:T(8,128)(2,1)} async-done(((bf16[64,1024]{1,0:T(8,128)(2,1)}), bf16[512,1024]{1,0:T(8,128)(2,1)}) %all-gather.11.cloned.1.call-update) | async-done | bytes 1048592 | tf_op jit(solution)/shard_map/all_gather | solution.py:59
  431.9 9.4 %reduce-scatter.3.cloned.1.call-done = bf16[512,176]{0,1:T(8,128)(2,1)} async-done(((bf16[1024,176]{0,1:T(8,128)(2,1)}), bf16[512,176]{0,1:T(8,128)(2,1)}) %reduce-scatter.3.cloned.1.call-update) | async-done | bytes 180240 | tf_op jit(solution)/shard_map/reduce_scatter | solution.py:112
  441.3 1.9 copy.48
  443.1 1.3 reshape.140
  445.2 1.9 all_gather.23
  447.2 2.8 fusion.38
  449.9 5.0 %copy.62 = bf16[2,8,110,1024]{3,2,1,0:T(8,128)(2,1)} copy(bf16[2,8,110,1024]{3,0,2,1:T(2,128)(2,1)} %all-to-all-done.4) | data formatting | bytes 7208960 | tf_op jit(solution)/shard_map/all_to_all | solution.py:103
  454.9 4.8 reshape.135
  459.7 9.7 %gather_fusion.1 = bf16[1408,1024]{1,0:T(8,128)(2,1)S(1)} fusion(bf16[1760,1024]{1,0:T(8,128)(2,1)} %reshape.135, s32[2048]{0:T(1024)S(1)} %pad_clamp_fusion), kind=kCustom, calls=%fused_computation.1 | custom fusion | bytes 5772800 | tf_op jit(solution)/shard_map/gather | solution.py:105
  469.4 1.7 fusion
  471.2 1.1 fusion.13
  472.3 1.3 copy.80
  473.6 1.0 copy-done.6
  474.6 1.3 copy.81
  476.0 0.6 copy-done.3
  476.6 1.0 copy.82
  477.6 0.6 copy-done.4
  478.2 1.0 copy.83
  479.2 1.0 copy.84
  (65 shorter events, 3.8 us)
Async XLA Ops:
  11.2 7.4 %copy-start.10 = (s32[176,8]{0,1:T(8,128)S(1)}, s32[176,8]{0,1:T(8,128)}, u32[]{:S(2)}) copy-start(s32[176,8]{0,1:T(8,128)} %param.11) | copy-start | bytes 16900
  11.2 7.8 %copy-start.5 = (bf16[176,2048]{1,0:T(8,128)(2,1)S(1)}, bf16[176,2048]{1,0:T(8,128)(2,1)}, u32[]{:S(2)}) copy-start(bf16[176,2048]{1,0:T(8,128)(2,1)} %param.10) | copy-start | bytes 2162692
  11.2 33.2 %all-to-all-start.1 = ((bf16[8,64,1024]{2,1,0:T(8,128)(2,1)}), bf16[8,64,1024]{2,1,0:T(8,128)(2,1)S(1)}, u32[]{:S(2)}, u32[]{:S(2)}) async-start(bf16[8,64,1024]{2,1,0:T(8,128)(2,1)} %get-tuple-element.41), calls=%async_computation.2 | async-start | bytes 2097152 | tf_op jit(solution)/shard_map/all_to_all | solution.py:40
  44.4 32.7 %all-to-all-start.2 = ((bf16[8,64,1024]{2,1,0:T(8,128)(2,1)}), bf16[8,64,1024]{2,1,0:T(8,128)(2,1)S(1)}, u32[]{:S(2)}, u32[]{:S(2)}) async-start(bf16[8,64,1024]{2,1,0:T(8,128)(2,1)} %get-tuple-element.42), calls=%async_computation.3 | async-start | bytes 2097152 | tf_op jit(solution)/shard_map/all_to_all | solution.py:41
  77.1 1.0 copy-start.1
  78.1 86.3 %all-to-all-start = ((bf16[2,8,110,1024]{3,0,2,1:T(2,128)(2,1)}), bf16[2,8,110,1024]{3,0,2,1:T(2,128)(2,1)}, u32[]{:S(2)}, u32[]{:S(2)}) async-start(bf16[2,8,110,1024]{3,0,2,1:T(2,128)(2,1)} %copy.55), calls=%async_computation.1 | async-start | bytes 7208960 | tf_op jit(solution)/shard_map/all_to_all | solution.py:77
  84.1 48.3 %all-gather.13.cloned.1.call-start = ((), (), s32[]{:S(2)}) async-start(), calls=%async_computation.11 | async-start | bytes 3145728 | tf_op jit(solution)/shard_map/all_gather | solution.py:50
  84.8 125.9 %reduce-scatter.5.cloned.1.call-start = ((), (), s32[]{:S(2)}) async-start(), calls=%async_computation.12 | async-start | bytes 5505024 | tf_op jit(solution)/shard_map/reduce_scatter | solution.py:84
  85.3 37.1 %collective-permute-start = (bf16[1,512,1024]{2,1,0:T(8,128)(2,1)S(1)}, bf16[1,512,1024]{2,1,0:T(8,128)(2,1)S(1)}, u32[]{:S(2)}, u32[]{:S(2)}) collective-permute-start(bf16[1,512,1024]{2,1,0:T(8,128)(2,1)S(1)} %bitcast.84), channel_id=1, source_target_pairs={{0,16},{16,0},{1,17},{17,1},{2,18},{18,2},{3,19},{19,3},{4,20},{20... | collective-permute-start | bytes 3145736 | tf_op jit(solution)/shard_map/ppermute | solution.py:46
  179.2 63.6 %all-gather.17.cloned.1.call-start = ((), (), s32[]{:S(2)}) async-start(), calls=%async_computation.14 | async-start | bytes 3145728 | tf_op jit(solution)/shard_map/all_gather | solution.py:51
  210.5 44.0 %all-gather.15.cloned.1.call-start = ((), (), s32[]{:S(2)}) async-start(), calls=%async_computation.13 | async-start | bytes 2703360 | tf_op jit(solution)/shard_map/all_gather | solution.py:98
  229.6 3.6 copy-start.7
  229.6 3.6 copy-start.8
  229.6 3.6 copy-start.12
  233.1 114.5 %all-gather.7.cloned.1.call-start = ((), (), s32[]{:S(2)}) async-start(), calls=%async_computation.7 | async-start | bytes 1179648 | tf_op jit(solution)/shard_map/all_gather | solution.py:57
  264.2 6.6 %copy-start.9 = (f32[64,1024]{1,0:T(8,128)S(1)}, f32[64,1024]{1,0:T(8,128)}, u32[]{:S(2)}) copy-start(f32[64,1024]{1,0:T(8,128)} %param.19) | copy-start | bytes 786436
  264.2 185.8 %all-to-all-start.4 = ((bf16[2,8,110,1024]{3,0,2,1:T(2,128)(2,1)}), bf16[2,8,110,1024]{3,0,2,1:T(2,128)(2,1)}, u32[]{:S(2)}, u32[]{:S(2)}) async-start(bf16[2,8,110,1024]{3,0,2,1:T(2,128)(2,1)} %bitcast.83), calls=%async_computation.6 | async-start | bytes 7208960 | tf_op jit(solution)/shard_map/all_to_all | solution.py:103
  270.1 120.1 %all-gather.9.cloned.1.call-start = ((), (), s32[]{:S(2)}) async-start(), calls=%async_computation.8 | async-start | bytes 1179648 | tf_op jit(solution)/shard_map/all_gather | solution.py:58
  270.7 161.3 %all-gather.11.cloned.1.call-start = ((), (), s32[]{:S(2)}) async-start(), calls=%async_computation.10 | async-start | bytes 1179648 | tf_op jit(solution)/shard_map/all_gather | solution.py:59
  271.4 169.9 %reduce-scatter.3.cloned.1.call-start = ((), (), s32[]{:S(2)}) async-start(), calls=%async_computation.9 | async-start | bytes 540672 | tf_op jit(solution)/shard_map/reduce_scatter | solution.py:112
  399.5 3.3 copy-start.11
  469.4 1.8 copy-start.2
  469.4 2.9 copy-start
  472.3 2.3 copy-start.6
  474.6 2.0 copy-start.3
  476.6 1.6 copy-start.4
Sparse Core Ops, SparseCore 0:
  87.0 45.3 all-gather.12
  179.3 10.9 reduce-scatter.4
  210.6 32.1 all-gather.16
  244.7 9.7 all-gather.14
  257.0 90.5 all-gather.6
  350.2 39.9 all-gather.8
  392.9 38.9 all-gather.10
  434.7 6.5 reduce-scatter.2
